TPU v7x, 32 devices: a whole 2x2x4 slice. The times are simulated.
32 devices in a mesh: fs: 8 (over z, x), tp: 4 (over y, core).
Axes of the slice: x: 2, y: 2, z: 4, core: 2. Of those that a mesh axis runs over, the one named last changes fastest.
Arguments:
- tokens: bfloat16 [6144, 2048], P('fs', 'tp'), may hold values from -6 to 6
- ffn_one_gain: float32 [2048], replicated, may hold values from 0.1 to 1.9
- ffn_one_gate: bfloat16 [2048, 5632], P('fs', 'tp'), may hold values from -0.125 to 0.125
- ffn_one_up: bfloat16 [2048, 5632], P('fs', 'tp'), may hold values from -0.125 to 0.125
- ffn_one_down: bfloat16 [5632, 2048], P('tp', 'fs'), may hold values from -0.078125 to 0.078125
- mix_gain: float32 [2048], replicated, may hold values from 0.1 to 1.9
- conv_value: bfloat16 [2048, 1024], P('fs', 'tp'), may hold values from -0.125 to 0.125
- conv_gate: bfloat16 [2048, 1024], P('fs', 'tp'), may hold values from -0.125 to 0.125
- conv_kernel: float32 [31, 1024], P(None, 'tp'), may hold values from -15 to 15
- conv_ln_gain: float32 [1024], P('tp'), may hold values from 0.1 to 1.9
- conv_out: bfloat16 [1024, 2048], P('tp', 'fs'), may hold values from -0.1875 to 0.1875
- ffn_two_gain: float32 [2048], replicated, may hold values from 0.1 to 1.9
- ffn_two_gate: bfloat16 [2048, 5632], P('fs', 'tp'), may hold values from -0.125 to 0.125
- ffn_two_up: bfloat16 [2048, 5632], P('fs', 'tp'), may hold values from -0.125 to 0.125
- ffn_two_down: bfloat16 [5632, 2048], P('tp', 'fs'), may hold values from -0.078125 to 0.078125
Outputs:
- layer_out: bfloat16 [6144, 2048], P('fs', 'tp')
All inputs are finite; a program needn't handle non-finite values.
Results may differ from a plain program's by a relative error of at most 0.017.
Values may be sent and summed in bfloat16 or wider, within the bound.
A program may use at most 128 MiB of HBM per device.

v0:
```python
from functools import partial

import jax
import jax.numpy as jnp
from jax import lax
from jax.sharding import PartitionSpec as P

CONV = 1024


def rms_rows(rows_in, gain_vec):
    values = rows_in.astype(jnp.float32)
    scaled = (
        values * lax.rsqrt(jnp.mean(values * values, axis=-1, keepdims=True) + 1e-06) * gain_vec
    )
    return scaled.astype(jnp.bfloat16)


def add_one(normed, running, shard_piece):
    columns = lax.slice_in_dim(normed, 0, shard_piece.shape[0], axis=1)
    return running + jnp.dot(columns, shard_piece, preferred_element_type=jnp.float32)


def add_two(normed, pieces):
    return (
        jnp.dot(normed, pieces[0], preferred_element_type=jnp.float32),
        jnp.dot(normed, pieces[1], preferred_element_type=jnp.float32),
    )


def ffn_terms(full_rows, gain_vec, w_gate, w_up, w_down):
    normed = rms_rows(full_rows, gain_vec)
    zero_carry = jnp.zeros((normed.shape[0], w_gate.shape[1]), jnp.float32)
    gate_pre = add_one(normed, zero_carry, lax.all_gather(w_gate, "fs", axis=0, tiled=True))
    up_pre = add_one(normed, zero_carry, lax.all_gather(w_up, "fs", axis=0, tiled=True))
    hidden = (jax.nn.silu(gate_pre) * up_pre).astype(jnp.bfloat16)
    return jnp.dot(
        hidden, lax.all_gather(w_down, "fs", axis=1, tiled=True), preferred_element_type=jnp.float32
    )


def conv_terms(full_rows, mix_gain, conv_value, conv_gate, conv_kernel, conv_ln_gain, conv_out):
    normed = rms_rows(full_rows, mix_gain)
    value_pre, gate_pre = add_two(
        normed,
        (
            lax.all_gather(conv_value, "fs", axis=0, tiled=True),
            lax.all_gather(conv_gate, "fs", axis=0, tiled=True),
        ),
    )
    gated_lin = value_pre * jax.nn.sigmoid(gate_pre)
    half_span = conv_kernel.shape[0] // 2
    convolved = lax.conv_general_dilated(
        gated_lin[None],
        conv_kernel[:, None, :],
        (1,),
        [(half_span, half_span)],
        dimension_numbers=("NWC", "WIO", "NWC"),
        feature_group_count=gated_lin.shape[1],
        precision=lax.Precision.HIGHEST,
    )[0]
    sum_one, sum_two = lax.psum(
        (jnp.sum(convolved, axis=1), jnp.sum(convolved * convolved, axis=1)), "tp"
    )
    mean_val = (sum_one / CONV)[:, None]
    varied = (sum_two / CONV)[:, None] - mean_val * mean_val
    active = jax.nn.silu((convolved - mean_val) * lax.rsqrt(varied + 1e-05) * conv_ln_gain).astype(
        jnp.bfloat16
    )
    return jnp.dot(
        active,
        lax.all_gather(conv_out, "fs", axis=1, tiled=True),
        preferred_element_type=jnp.float32,
    )


def per_device(
    tokens,
    ffn_one_gain,
    ffn_one_gate,
    ffn_one_up,
    ffn_one_down,
    mix_gain,
    conv_value,
    conv_gate,
    conv_kernel,
    conv_ln_gain,
    conv_out,
    ffn_two_gain,
    ffn_two_gate,
    ffn_two_up,
    ffn_two_down,
):
    sublayers = [
        (
            partial(
                ffn_terms,
                gain_vec=ffn_one_gain,
                w_gate=ffn_one_gate,
                w_up=ffn_one_up,
                w_down=ffn_one_down,
            ),
            0.5,
        ),
        (
            partial(
                conv_terms,
                mix_gain=mix_gain,
                conv_value=conv_value,
                conv_gate=conv_gate,
                conv_kernel=conv_kernel,
                conv_ln_gain=conv_ln_gain,
                conv_out=conv_out,
            ),
            1.0,
        ),
        (
            partial(
                ffn_terms,
                gain_vec=ffn_two_gain,
                w_gate=ffn_two_gate,
                w_up=ffn_two_up,
                w_down=ffn_two_down,
            ),
            0.5,
        ),
    ]
    current = tokens
    for sublayer, factor in sublayers:
        full_rows = lax.all_gather(current, "tp", axis=1, tiled=True)
        summed = lax.psum_scatter(
            sublayer(full_rows).astype(jnp.bfloat16), "tp", scatter_dimension=1, tiled=True
        ).astype(jnp.float32)
        current = (current.astype(jnp.float32) + factor * summed).astype(jnp.bfloat16)
    return current


def solution(mesh):
    in_specs = (
        P("fs", "tp"),
        P(),
        P("fs", "tp"),
        P("fs", "tp"),
        P("tp", "fs"),
        P(),
        P("fs", "tp"),
        P("fs", "tp"),
        P(None, "tp"),
        P("tp"),
        P("tp", "fs"),
        P(),
        P("fs", "tp"),
        P("fs", "tp"),
        P("tp", "fs"),
    )
    out_specs = P("fs", "tp")
    return jax.shard_map(
        per_device, mesh=mesh, in_specs=in_specs, out_specs=out_specs, check_vma=False
    )
```

profile of v0, /device:TPU:0, one launch (start us, length us, event | category | flops | bytes accessed | tf_op | source)
XLA Modules:
  0.0 943.1 jit_solution(7540141789120171966)
XLA Ops:
  6.5 0.7 all-gather.13.cloned.1.call-update
  7.3 0.7 all-gather.15.cloned.1.call-update
  8.1 0.7 all-gather.17.cloned.1.call-update
  8.8 0.5 all-gather.19.cloned.1.call-update
  9.4 30.8 %all-gather.13.cloned.1.call-done = bf16[768,2048]{1,0:T(8,128)(2,1)} async-done(((bf16[768,512]{1,0:T(8,128)(2,1)}), bf16[768,2048]{1,0:T(8,128)(2,1)}) %all-gather.13.cloned.1.call-update) | async-done | bytes 3145744 | tf_op jit(solution)/shard_map/all_gather | solution.py:130
  40.2 2.6 fusion
  42.8 91.9 %all-gather.15.cloned.1.call-done = bf16[2048,1408]{1,0:T(8,128)(2,1)} async-done(((bf16[256,1408]{1,0:T(8,128)(2,1)}), bf16[2048,1408]{1,0:T(8,128)(2,1)}) %all-gather.15.cloned.1.call-update) | async-done | bytes 5767184 | tf_op jit(solution)/shard_map/all_gather | solution.py:34
  134.7 9.9 %fusion.23 = f32[768,1408]{1,0:T(8,128)} fusion(bf16[2048,1408]{1,0:T(8,128)(2,1)} %all-gather.15.cloned.1.call-done, bf16[768,2048]{1,0:T(8,128)(2,1)} %all-gather.13.cloned.1.call-done, f32[2048]{0:T(1024)S(1)} %copy-done.6, f32[768]{0:T(1024)S(1)} %add_rsqrt_fusion.3), kind=kOutput, calls=%fused_computation.36 | convolution fusion | flops 4435476480 | bytes 13249536 | tf_op jit(solution)/shard_map/dot_general | solution.py:21
  144.6 82.8 %all-gather.17.cloned.1.call-done = bf16[2048,1408]{1,0:T(8,128)(2,1)} async-done(((bf16[256,1408]{1,0:T(8,128)(2,1)}), bf16[2048,1408]{1,0:T(8,128)(2,1)}) %all-gather.17.cloned.1.call-update) | async-done | bytes 5767184 | tf_op jit(solution)/shard_map/all_gather | solution.py:35
  227.4 93.2 %all-gather.19.cloned.1.call-done = bf16[1408,2048]{1,0:T(8,128)(2,1)} async-done(((bf16[1408,256]{1,0:T(8,128)(2,1)}), bf16[1408,2048]{1,0:T(8,128)(2,1)}) %all-gather.19.cloned.1.call-update) | async-done | bytes 5767184 | tf_op jit(solution)/shard_map/all_gather | solution.py:38
  320.6 17.4 %convolution_convert_fusion.2 = bf16[768,2048]{1,0:T(8,128)(2,1)} fusion(bf16[1408,2048]{1,0:T(8,128)(2,1)} %all-gather.19.cloned.1.call-done, f32[768,1408]{1,0:T(8,128)} %fusion.23, bf16[2048,1408]{1,0:T(8,128)(2,1)} %all-gather.17.cloned.1.call-done, bf16[768,2048]{1,0:T(8,128)(2,1)S(1)} %copy-done.4, f32[2048]{0:T(1024)S(1)} %copy-done.6, ...), kind=kOutput, calls=%fused_computation.19 | convolution fusion | flops 8872722432 | bytes 22162432 | tf_op jit(solution)/shard_map/dot_general | solution.py:37
  338.1 36.0 %reduce-scatter.4.cloned.1.call-done = bf16[768,512]{1,0:T(8,128)(2,1)} async-done(((bf16[768,2048]{1,0:T(8,128)(2,1)}), bf16[768,512]{1,0:T(8,128)(2,1)}) %reduce-scatter.4.cloned.1.call-update) | async-done | bytes 786448 | tf_op jit(solution)/shard_map/reduce_scatter | solution.py:131
  374.1 2.5 add_convert_fusion.2
  376.6 0.7 all-gather.25.cloned.1.call-update
  377.4 0.7 all-gather.23.cloned.1.call-update
  378.1 0.7 all-gather.27.cloned.1.call-update
  378.8 0.2 reduce-scatter.6.cloned.1.call-start
  379.0 26.2 %all-gather.21.cloned.1.call-done = bf16[768,2048]{1,0:T(8,128)(2,1)} async-done(((bf16[768,512]{1,0:T(8,128)(2,1)}), bf16[768,2048]{1,0:T(8,128)(2,1)}) %all-gather.21.cloned.1.call-update) | async-done | bytes 3145744 | tf_op jit(solution)/shard_map/all_gather | solution.py:130
  405.2 2.6 fusion.3
  407.8 39.8 %all-gather.25.cloned.1.call-done = bf16[2048,256]{1,0:T(8,128)(2,1)} async-done(((bf16[256,256]{1,0:T(8,128)(2,1)}), bf16[2048,256]{1,0:T(8,128)(2,1)}) %all-gather.25.cloned.1.call-update) | async-done | bytes 1048592 | tf_op jit(solution)/shard_map/all_gather | solution.py:48
  447.7 4.1 fusion.12
  451.8 37.0 %all-gather.23.cloned.1.call-done = bf16[2048,256]{1,0:T(8,128)(2,1)} async-done(((bf16[256,256]{1,0:T(8,128)(2,1)}), bf16[2048,256]{1,0:T(8,128)(2,1)}) %all-gather.23.cloned.1.call-update) | async-done | bytes 1048592 | tf_op jit(solution)/shard_map/all_gather | solution.py:47
  488.8 2.5 fusion.10
  491.4 0.1 reshape.36
  491.5 0.3 copy.21
  491.8 0.2 copy-done.10
  492.0 1.7 convolution_select_fusion
  493.8 0.3 copy.23
  494.1 0.2 slice_reduce_fusion
  494.3 0.2 fusion.31
  494.5 5.8 all-reduce
  500.3 28.7 %all-gather.27.cloned.1.call-done = bf16[256,2048]{1,0:T(8,128)(2,1)} async-done(((bf16[256,256]{1,0:T(8,128)(2,1)}), bf16[256,2048]{1,0:T(8,128)(2,1)}) %all-gather.27.cloned.1.call-update) | async-done | bytes 1048592 | tf_op jit(solution)/shard_map/all_gather | solution.py:72
  529.0 4.0 convolution_convert_fusion
  533.1 36.8 %reduce-scatter.6.cloned.1.call-done = bf16[768,512]{1,0:T(8,128)(2,1)} async-done(((bf16[768,2048]{1,0:T(8,128)(2,1)}), bf16[768,512]{1,0:T(8,128)(2,1)}) %reduce-scatter.6.cloned.1.call-update) | async-done | bytes 786448 | tf_op jit(solution)/shard_map/reduce_scatter | solution.py:131
  570.0 2.2 add_convert_fusion.1
  572.3 0.5 all-gather.31.cloned.1.call-update
  572.8 0.7 all-gather.33.cloned.1.call-update
  573.6 0.5 all-gather.35.cloned.1.call-update
  574.1 0.3 reduce-scatter.8.cloned.1.call-start
  574.4 26.5 %all-gather.29.cloned.1.call-done = bf16[768,2048]{1,0:T(8,128)(2,1)} async-done(((bf16[768,512]{1,0:T(8,128)(2,1)}), bf16[768,2048]{1,0:T(8,128)(2,1)}) %all-gather.29.cloned.1.call-update) | async-done | bytes 3145744 | tf_op jit(solution)/shard_map/all_gather | solution.py:130
  600.9 2.6 fusion.6
  603.5 91.8 %all-gather.31.cloned.1.call-done = bf16[2048,1408]{1,0:T(8,128)(2,1)} async-done(((bf16[256,1408]{1,0:T(8,128)(2,1)}), bf16[2048,1408]{1,0:T(8,128)(2,1)}) %all-gather.31.cloned.1.call-update) | async-done | bytes 5767184 | tf_op jit(solution)/shard_map/all_gather | solution.py:34
  695.3 9.9 %fusion.18 = f32[768,1408]{1,0:T(8,128)} fusion(bf16[2048,1408]{1,0:T(8,128)(2,1)} %all-gather.31.cloned.1.call-done, bf16[768,2048]{1,0:T(8,128)(2,1)} %all-gather.29.cloned.1.call-done, f32[2048]{0:T(1024)S(1)} %copy-done.8, f32[768]{0:T(1024)S(1)} %add_rsqrt_fusion), kind=kOutput, calls=%fused_computation.35 | convolution fusion | flops 4435476480 | bytes 13249536 | tf_op jit(solution)/shard_map/dot_general | solution.py:21
  705.2 82.8 %all-gather.33.cloned.1.call-done = bf16[2048,1408]{1,0:T(8,128)(2,1)} async-done(((bf16[256,1408]{1,0:T(8,128)(2,1)}), bf16[2048,1408]{1,0:T(8,128)(2,1)}) %all-gather.33.cloned.1.call-update) | async-done | bytes 5767184 | tf_op jit(solution)/shard_map/all_gather | solution.py:35
  788.0 93.2 %all-gather.35.cloned.1.call-done = bf16[1408,2048]{1,0:T(8,128)(2,1)} async-done(((bf16[1408,256]{1,0:T(8,128)(2,1)}), bf16[1408,2048]{1,0:T(8,128)(2,1)}) %all-gather.35.cloned.1.call-update) | async-done | bytes 5767184 | tf_op jit(solution)/shard_map/all_gather | solution.py:38
  881.2 17.0 %convolution_convert_fusion.1 = bf16[768,2048]{1,0:T(8,128)(2,1)} fusion(bf16[1408,2048]{1,0:T(8,128)(2,1)} %all-gather.35.cloned.1.call-done, f32[768,1408]{1,0:T(8,128)} %fusion.18, bf16[2048,1408]{1,0:T(8,128)(2,1)} %all-gather.33.cloned.1.call-done, bf16[768,2048]{1,0:T(8,128)(2,1)} %all-gather.29.cloned.1.call-done, f32[2048]{0:T(1024)S(1)} %copy-done.8, ...), kind=kOutput, calls=%fused_computation.18 | convolution fusion | flops 8872722432 | bytes 22162432 | tf_op jit(solution)/shard_map/dot_general | solution.py:37
  898.2 36.1 %reduce-scatter.8.cloned.1.call-done = bf16[768,512]{1,0:T(8,128)(2,1)} async-done(((bf16[768,2048]{1,0:T(8,128)(2,1)}), bf16[768,512]{1,0:T(8,128)(2,1)}) %reduce-scatter.8.cloned.1.call-update) | async-done | bytes 786448 | tf_op jit(solution)/shard_map/reduce_scatter | solution.py:131
  934.3 2.2 add_convert_fusion
  (46 shorter events, 0.8 us)
Async XLA Ops:
  6.5 485.3 %copy-start = (f32[31,256]{1,0:T(8,128)S(1)}, f32[31,256]{1,0:T(8,128)}, u32[]{:S(2)}) copy-start(f32[31,256]{1,0:T(8,128)} %param.23) | copy-start | bytes 95236
  6.5 128.1 %copy-start.6 = (f32[2048]{0:T(1024)S(1)}, f32[2048]{0:T(1024)}, u32[]{:S(2)}) copy-start(f32[2048]{0:T(1024)} %param.16) | copy-start | bytes 24580
  6.5 33.6 %all-gather.13.cloned.1.call-start = ((), (), s32[]{:S(2)}) async-start(), calls=%async_computation.3 | async-start | bytes 3932160 | tf_op jit(solution)/shard_map/all_gather | solution.py:130
  7.3 127.4 %all-gather.15.cloned.1.call-start = ((), (), s32[]{:S(2)}) async-start(), calls=%async_computation.4 | async-start | bytes 6488064 | tf_op jit(solution)/shard_map/all_gather | solution.py:34
  8.0 219.4 %all-gather.17.cloned.1.call-start = ((), (), s32[]{:S(2)}) async-start(), calls=%async_computation.5 | async-start | bytes 6488064 | tf_op jit(solution)/shard_map/all_gather | solution.py:35
  8.7 311.9 %all-gather.19.cloned.1.call-start = ((), (), s32[]{:S(2)}) async-start(), calls=%async_computation.6 | async-start | bytes 6488064 | tf_op jit(solution)/shard_map/all_gather | solution.py:38
  9.3 364.8 %reduce-scatter.4.cloned.1.call-start = ((), (), s32[]{:S(2)}) async-start(), calls=%async_computation.7 | async-start | bytes 3932160 | tf_op jit(solution)/shard_map/reduce_scatter | solution.py:131
  42.7 277.9 %copy-start.4 = (bf16[768,2048]{1,0:T(8,128)(2,1)S(1)}, bf16[768,2048]{1,0:T(8,128)(2,1)}, u32[]{:S(2)}) copy-start(bf16[768,2048]{1,0:T(8,128)(2,1)} %all-gather.13.cloned.1.call-done) | copy-start | bytes 9437188
  338.0 109.7 %copy-start.7 = (f32[2048]{0:T(1024)S(1)}, f32[2048]{0:T(1024)}, u32[]{:S(2)}) copy-start(f32[2048]{0:T(1024)} %param.20) | copy-start | bytes 24580
  338.0 67.2 %all-gather.21.cloned.1.call-start = ((), (), s32[]{:S(2)}) async-start(), calls=%async_computation.8 | async-start | bytes 3932160 | tf_op jit(solution)/shard_map/all_gather | solution.py:130
  376.6 71.1 %all-gather.25.cloned.1.call-start = ((), (), s32[]{:S(2)}) async-start(), calls=%async_computation.10 | async-start | bytes 1179648 | tf_op jit(solution)/shard_map/all_gather | solution.py:48
  377.3 111.5 %all-gather.23.cloned.1.call-start = ((), (), s32[]{:S(2)}) async-start(), calls=%async_computation.9 | async-start | bytes 1179648 | tf_op jit(solution)/shard_map/all_gather | solution.py:47
  378.1 150.9 %all-gather.27.cloned.1.call-start = ((), (), s32[]{:S(2)}) async-start(), calls=%async_computation.11 | async-start | bytes 1179648 | tf_op jit(solution)/shard_map/all_gather | solution.py:72
  378.8 191.1 %reduce-scatter.6.cloned.1.call-start = ((), (), s32[]{:S(2)}) async-start(), calls=%async_computation.12 | async-start | bytes 3932160 | tf_op jit(solution)/shard_map/reduce_scatter | solution.py:131
  407.8 81.0 %copy-start.5 = (bf16[768,2048]{1,0:T(8,128)(2,1)S(1)}, bf16[768,2048]{1,0:T(8,128)(2,1)}, u32[]{:S(2)}) copy-start(bf16[768,2048]{1,0:T(8,128)(2,1)} %all-gather.21.cloned.1.call-done) | copy-start | bytes 9437188
  491.3 0.7 copy-start.10
  493.8 35.3 %copy-start.9 = (f32[256]{0:T(256)S(1)}, f32[256]{0:T(256)}, u32[]{:S(2)}) copy-start(f32[256]{0:T(256)} %param.24) | copy-start | bytes 3076
  529.0 40.9 %copy-start.2 = (bf16[768,512]{1,0:T(8,128)(2,1)S(1)}, bf16[768,512]{1,0:T(8,128)(2,1)}, u32[]{:S(2)}) copy-start(bf16[768,512]{1,0:T(8,128)(2,1)} %add_convert_fusion.2) | copy-start | bytes 2359300
  533.1 162.2 %copy-start.8 = (f32[2048]{0:T(1024)S(1)}, f32[2048]{0:T(1024)}, u32[]{:S(2)}) copy-start(f32[2048]{0:T(1024)} %param.26) | copy-start | bytes 24580
  533.1 67.8 %all-gather.29.cloned.1.call-start = ((), (), s32[]{:S(2)}) async-start(), calls=%async_computation.13 | async-start | bytes 3932160 | tf_op jit(solution)/shard_map/all_gather | solution.py:130
  572.2 123.0 %all-gather.31.cloned.1.call-start = ((), (), s32[]{:S(2)}) async-start(), calls=%async_computation.14 | async-start | bytes 6488064 | tf_op jit(solution)/shard_map/all_gather | solution.py:34
  572.8 215.2 %all-gather.33.cloned.1.call-start = ((), (), s32[]{:S(2)}) async-start(), calls=%async_computation.15 | async-start | bytes 6488064 | tf_op jit(solution)/shard_map/all_gather | solution.py:35
  573.5 307.7 %all-gather.35.cloned.1.call-start = ((), (), s32[]{:S(2)}) async-start(), calls=%async_computation.16 | async-start | bytes 6488064 | tf_op jit(solution)/shard_map/all_gather | solution.py:38
  574.1 360.2 %reduce-scatter.8.cloned.1.call-start = ((), (), s32[]{:S(2)}) async-start(), calls=%async_computation.17 | async-start | bytes 3932160 | tf_op jit(solution)/shard_map/reduce_scatter | solution.py:131
  705.2 229.1 %copy-start.3 = (bf16[768,512]{1,0:T(8,128)(2,1)S(1)}, bf16[768,512]{1,0:T(8,128)(2,1)}, u32[]{:S(2)}) copy-start(bf16[768,512]{1,0:T(8,128)(2,1)} %add_convert_fusion.1) | copy-start | bytes 2359300
  881.2 55.3 %copy-start.1 = (f32[31,256]{1,0:T(8,128)S(1)}, f32[31,256]{1,0:T(8,128)}, u32[]{:S(2)}) copy-start(f32[31,256]{1,0:T(8,128)} %param.23) | copy-start | bytes 95236
Sparse Core Ops, SparseCore 0:
  8.9 31.2 all-gather.12
  42.3 92.2 all-gather.14
  136.9 90.4 all-gather.16
  229.3 91.2 all-gather.18
  338.1 35.8 reduce-scatter.3
  376.7 28.4 all-gather.20
  407.4 40.2 all-gather.24
  449.8 38.9 all-gather.22
  490.9 38.0 all-gather.26
  533.2 36.7 reduce-scatter.5
  572.3 28.5 all-gather.28
  602.9 92.2 all-gather.30
  697.4 90.4 all-gather.32
  789.9 91.2 all-gather.34
  898.3 35.9 reduce-scatter.7
where the time goes:
time: 944 us; the launch traced here: 943 us
  waiting for transfers between devices  840 us (89%)
  matrix products  66.6 us (7%)
  other arithmetic  15 us (2%)
  between operations  13.5 us (1%)
    all_gather x2, waiting for transfers between devices, ffn_terms(): lax.all_gather(w_down, 'fs', axis=1, tiled=True)  186 us
    all_gather x2, waiting for transfers between devices, ffn_terms(): lax.all_gather(w_gate, 'fs', axis=0, tiled=True)  184 us
    all_gather x2, waiting for transfers between devices, ffn_terms(): lax.all_gather(w_up, 'fs', axis=0, tiled=True)  166 us
    reduce_scatter x3, waiting for transfers between devices, per_device(): lax.psum_scatter(sublayer(full_rows).astype(jnp.bfloat16), 'tp', scatter_...  109 us
    all_gather x3, waiting for transfers between devices, per_device(): full_rows = lax.all_gather(current, 'tp', axis=1, tiled=True)  83.5 us
    all_gather x1, waiting for transfers between devices, conv_terms(): lax.all_gather(conv_gate, 'fs', axis=0, tiled=True)  39.8 us
    all_gather x1, waiting for transfers between devices, conv_terms(): lax.all_gather(conv_value, 'fs', axis=0, tiled=True)  37 us
    dot_general x2, matrix products, ffn_terms(): jnp.dot(hidden, lax.all_gather(w_down, 'fs', axis=1, tiled=True), preferr...  34.3 us
  transfers between devices with their start and end apart: 15, of which 15 were waited for; matrix products, arithmetic and copies ran while one was open for 4% of the time, Pallas kernels for 0%

commit v1 on v0

v1 whole, which is shorter than its diff:
```python
from functools import partial

import jax
import jax.numpy as jnp
from jax import lax
from jax.sharding import PartitionSpec as P


def rms_rows(rows_in, gain_vec):
    values = rows_in.astype(jnp.float32)
    scaled = (
        values * lax.rsqrt(jnp.mean(values * values, axis=-1, keepdims=True) + 1e-06) * gain_vec
    )
    return scaled.astype(jnp.bfloat16)


def split_fs():
    total = lax.axis_size("fs")
    inner = 1
    while total % (inner * 2) == 0 and (inner * 2) ** 2 <= total:
        inner *= 2
    return total // inner, inner


def spread_blocks(shard):
    outer, inner = split_fs()
    me = lax.axis_index("fs")
    mine_z, mine_x = me // inner, me % inner
    held = [shard]
    for hop in range(1, outer):
        pairs = [
            (z * inner + x, ((z + hop) % outer) * inner + x)
            for z in range(outer)
            for x in range(inner)
        ]
        held.append(lax.ppermute(shard, "fs", pairs))
    blocks = []
    for hop, block in enumerate(held):
        blocks.append((((mine_z - hop) % outer) * inner + mine_x, block))
        for step in range(1, inner):
            pairs = [
                (z * inner + x, z * inner + (x + step) % inner)
                for z in range(outer)
                for x in range(inner)
            ]
            owner = ((mine_z - hop) % outer) * inner + (mine_x - step) % inner
            blocks.append((owner, lax.ppermute(block, "fs", pairs)))
    return blocks


def place_blocks(blocks, axis):
    shape = list(blocks[0][1].shape)
    width = shape[axis]
    shape[axis] = width * len(blocks)
    whole = jnp.zeros(shape, blocks[0][1].dtype)
    for owner, block in blocks:
        whole = lax.dynamic_update_slice_in_dim(whole, block, owner * width, axis)
    return whole


def down_product(hidden, blocks):
    return place_blocks(
        [
            (
                owner,
                jnp.dot(hidden, block, preferred_element_type=jnp.float32).astype(jnp.bfloat16),
            )
            for owner, block in blocks
        ],
        1,
    )


def ffn_terms(full_rows, gain_vec, gate_blocks, up_blocks, down_blocks):
    normed = rms_rows(full_rows, gain_vec)
    gate_pre = jnp.dot(normed, place_blocks(gate_blocks, 0), preferred_element_type=jnp.float32)
    up_pre = jnp.dot(normed, place_blocks(up_blocks, 0), preferred_element_type=jnp.float32)
    hidden = (jax.nn.silu(gate_pre) * up_pre).astype(jnp.bfloat16)
    return down_product(hidden, down_blocks)


def conv_terms(full_rows, mix_gain, conv_blocks, conv_kernel, conv_ln_gain):
    normed = rms_rows(full_rows, mix_gain)
    value_whole = place_blocks([(owner, block[0]) for owner, block in conv_blocks], 0)
    gate_whole = place_blocks([(owner, block[1]) for owner, block in conv_blocks], 0)
    value_pre = jnp.dot(normed, value_whole, preferred_element_type=jnp.float32)
    gate_pre = jnp.dot(normed, gate_whole, preferred_element_type=jnp.float32)
    gated_lin = value_pre * jax.nn.sigmoid(gate_pre)
    half_span = conv_kernel.shape[0] // 2
    convolved = lax.conv_general_dilated(
        gated_lin[None],
        conv_kernel[:, None, :],
        (1,),
        [(half_span, half_span)],
        dimension_numbers=("NWC", "WIO", "NWC"),
        feature_group_count=gated_lin.shape[1],
        precision=lax.Precision.HIGHEST,
    )[0]
    sum_one, sum_two = lax.psum(
        (jnp.sum(convolved, axis=1), jnp.sum(convolved * convolved, axis=1)), "tp"
    )
    channels = convolved.shape[1] * lax.axis_size("tp")
    mean_val = (sum_one / channels)[:, None]
    varied = (sum_two / channels)[:, None] - mean_val * mean_val
    active = jax.nn.silu((convolved - mean_val) * lax.rsqrt(varied + 1e-05) * conv_ln_gain).astype(
        jnp.bfloat16
    )
    out_whole = place_blocks([(owner, block[2]) for owner, block in conv_blocks], 0)
    return jnp.einsum("tc,dc->td", active, out_whole, preferred_element_type=jnp.float32)


def keep_features(terms):
    outer = lax.axis_size("tp") // 2
    width = terms.shape[1] // (2 * outer)
    me = lax.axis_index("tp")
    mine_y, core = me // 2, me % 2

    def piece(y, half):
        return lax.dynamic_slice_in_dim(terms, (y * 2 + half) * width, width, 1)

    swap = [(d, d ^ 1) for d in range(2 * outer)]
    halves = []
    for hop in range(outer):
        target = (mine_y + hop) % outer
        other = lax.ppermute(piece(target, 1 - core), "tp", swap)
        halves.append(piece(target, core).astype(jnp.float32) + other.astype(jnp.float32))
    total = halves[0]
    for hop in range(1, outer):
        pairs = [
            (y * 2 + half, ((y + hop) % outer) * 2 + half)
            for y in range(outer)
            for half in range(2)
        ]
        arrived = lax.ppermute(halves[hop].astype(jnp.bfloat16), "tp", pairs)
        total = total + arrived.astype(jnp.float32)
    return total


def per_device(
    tokens,
    ffn_one_gain,
    ffn_one_gate,
    ffn_one_up,
    ffn_one_down,
    mix_gain,
    conv_value,
    conv_gate,
    conv_kernel,
    conv_ln_gain,
    conv_out,
    ffn_two_gain,
    ffn_two_gate,
    ffn_two_up,
    ffn_two_down,
):
    conv_pack = jnp.stack((conv_value, conv_gate, conv_out.T))
    sublayers = [
        (
            partial(
                ffn_terms,
                gain_vec=ffn_one_gain,
                gate_blocks=spread_blocks(ffn_one_gate),
                up_blocks=spread_blocks(ffn_one_up),
                down_blocks=spread_blocks(ffn_one_down),
            ),
            0.5,
        ),
        (
            partial(
                conv_terms,
                mix_gain=mix_gain,
                conv_blocks=spread_blocks(conv_pack),
                conv_kernel=conv_kernel,
                conv_ln_gain=conv_ln_gain,
            ),
            1.0,
        ),
        (
            partial(
                ffn_terms,
                gain_vec=ffn_two_gain,
                gate_blocks=spread_blocks(ffn_two_gate),
                up_blocks=spread_blocks(ffn_two_up),
                down_blocks=spread_blocks(ffn_two_down),
            ),
            0.5,
        ),
    ]
    current = tokens
    for sublayer, factor in sublayers:
        full_rows = lax.all_gather(current, "tp", axis=1, tiled=True)
        run = sublayer
        summed = keep_features(run(full_rows).astype(jnp.bfloat16))
        current = (current.astype(jnp.float32) + factor * summed).astype(jnp.bfloat16)
    return current


def solution(mesh):
    in_specs = (
        P("fs", "tp"),
        P(),
        P("fs", "tp"),
        P("fs", "tp"),
        P("tp", "fs"),
        P(),
        P("fs", "tp"),
        P("fs", "tp"),
        P(None, "tp"),
        P("tp"),
        P("tp", "fs"),
        P(),
        P("fs", "tp"),
        P("fs", "tp"),
        P("tp", "fs"),
    )
    out_specs = P("fs", "tp")
    return jax.shard_map(
        per_device, mesh=mesh, in_specs=in_specs, out_specs=out_specs, check_vma=False
    )
```

time: 944 us -> 674 us (0.71)
  the two profiles are of different devices: /device:TPU:0 before, /device:TPU:12 now
where the time goes in v1:
time: 674 us; the launch traced here: 670 us
  waiting for transfers between devices  473 us (70%)
  matrix products  62.6 us (9%)
  local copies, waits for them, and re-layouts  50.1 us (7%)
  starting transfers between devices  47.8 us (7%)
  other arithmetic  17.2 us (3%)
  between operations  14 us (2%)
    ppermute x21, waiting for transfers between devices, spread_blocks(): held.append(lax.ppermute(shard, 'fs', pairs))  280 us
    ppermute x28, waiting for transfers between devices, spread_blocks(): blocks.append((owner, lax.ppermute(block, 'fs', pairs)))  129 us
    ppermute x3, waiting for transfers between devices, keep_features(): arrived = lax.ppermute(halves[hop].astype(jnp.bfloat16), 'tp', pairs)  57 us
    dynamic_update_slice x42, local copies, waits for them, and re-layouts, place_blocks(): whole = lax.dynamic_update_slice_in_dim(whole, block, owner * width, axis)  33.2 us
    dot_general x16, matrix products, down_product(): jnp.dot(hidden, block, preferred_element_type=jnp.float32)  25.7 us
    ppermute x28, starting transfers between devices, spread_blocks(): blocks.append((owner, lax.ppermute(block, 'fs', pairs)))  25 us
    ppermute x21, starting transfers between devices, spread_blocks(): held.append(lax.ppermute(shard, 'fs', pairs))  19.7 us
    dot_general x2, matrix products, ffn_terms(): jnp.dot(normed, place_blocks(up_blocks, 0), preferred_element_type=jnp.fl...  16.5 us
  transfers between devices with their start and end apart: 61, of which 38 were waited for; matrix products, arithmetic and copies ran while one was open for 16% of the time, Pallas kernels for 0%

profile of v1, /device:TPU:12, one launch (start us, length us, event | category | flops | bytes accessed | tf_op | source)
XLA Modules:
  0.0 670.4 jit_solution(7494568070588187624)
XLA Ops:
  12.9 2.9 broadcast.87.clone.1
  16.7 3.0 broadcast.87.clone.2
  20.7 6.0 collective-permute-done
  27.2 15.2 %collective-permute-done.1 = bf16[256,1408]{1,0:T(8,128)(2,1)S(1)} collective-permute-done((bf16[256,1408]{1,0:T(8,128)(2,1)}, bf16[256,1408]{1,0:T(8,128)(2,1)S(1)}, u32[]{:S(2)}, u32[]{:S(2)}) %collective-permute-start.1) | collective-permute-done | bytes 720928 | tf_op jit(solution)/shard_map/ppermute | solution.py:36
  45.8 74.2 %collective-permute-done.8 = bf16[256,1408]{1,0:T(8,128)(2,1)S(1)} collective-permute-done((bf16[256,1408]{1,0:T(8,128)(2,1)}, bf16[256,1408]{1,0:T(8,128)(2,1)S(1)}, u32[]{:S(2)}, u32[]{:S(2)}) %collective-permute-start.8) | collective-permute-done | bytes 720928 | tf_op jit(solution)/shard_map/ppermute | solution.py:36
  127.0 7.6 %collective-permute-done.10 = bf16[256,1408]{1,0:T(8,128)(2,1)S(1)} collective-permute-done((bf16[256,1408]{1,0:T(8,128)(2,1)S(1)}, bf16[256,1408]{1,0:T(8,128)(2,1)S(1)}, u32[]{:S(2)}, u32[]{:S(2)}) %collective-permute-start.10) | collective-permute-done | bytes 720928 | tf_op jit(solution)/shard_map/ppermute | solution.py:36
  134.7 4.4 collective-permute-done.9
  141.4 13.0 %collective-permute-done.4 = bf16[256,1408]{1,0:T(8,128)(2,1)S(1)} collective-permute-done((bf16[256,1408]{1,0:T(8,128)(2,1)S(1)}, bf16[256,1408]{1,0:T(8,128)(2,1)S(1)}, u32[]{:S(2)}, u32[]{:S(2)}) %collective-permute-start.4) | collective-permute-done | bytes 720928 | tf_op jit(solution)/shard_map/ppermute | solution.py:47
  155.4 4.3 collective-permute-start.19
  161.1 8.8 %collective-permute-done.11 = bf16[256,1408]{1,0:T(8,128)(2,1)S(1)} collective-permute-done((bf16[256,1408]{1,0:T(8,128)(2,1)S(1)}, bf16[256,1408]{1,0:T(8,128)(2,1)S(1)}, u32[]{:S(2)}, u32[]{:S(2)}) %collective-permute-start.11) | collective-permute-done | bytes 720928 | tf_op jit(solution)/shard_map/ppermute | solution.py:47
  173.8 22.1 %collective-permute-done.17 = bf16[1408,256]{1,0:T(8,128)(2,1)} collective-permute-done((bf16[1408,256]{1,0:T(8,128)(2,1)}, bf16[1408,256]{1,0:T(8,128)(2,1)}, u32[]{:S(2)}, u32[]{:S(2)}) %collective-permute-start.17) | collective-permute-done | bytes 720928 | tf_op jit(solution)/shard_map/ppermute | solution.py:36
  196.4 6.0 collective-permute-done.19
  206.3 2.7 fusion
  209.1 7.6 %fusion.41 = f32[768,1408]{1,0:T(8,128)S(1)} fusion(bf16[2048,1408]{1,0:T(8,128)(2,1)} %constant_dynamic-update-slice_fusion.26, bf16[768,2048]{1,0:T(8,128)(2,1)S(1)} %copy-done.4, f32[2048]{0:T(1024)S(1)} %copy-done.14, f32[768]{0:T(1024)S(1)} %add_rsqrt_fusion.3), kind=kOutput, calls=%fused_computation.71 | convolution fusion | flops 4435476480 | bytes 13249536 | tf_op jit(solution)/shard_map/dot_general | solution.py:76
  216.7 8.2 %multiply_convert_fusion.1 = bf16[768,1408]{1,0:T(8,128)(2,1)S(1)} fusion(f32[768,1408]{1,0:T(8,128)S(1)} %fusion.41, bf16[2048,1408]{1,0:T(8,128)(2,1)} %constant_dynamic-update-slice_fusion.18, bf16[768,2048]{1,0:T(8,128)(2,1)S(1)} %copy-done.4, f32[2048]{0:T(1024)S(1)} %copy-done.14, f32[768]{0:T(1024)S(1)} %add_rsqrt_fusion.3), kind=kOutput, calls=%fused_computation.16 | convolution fusion | flops 4441964544 | bytes 15412224 | tf_op jit(solution)/shard_map/dot_general | solution.py:77
  235.6 11.7 %collective-permute-done.18 = bf16[1408,256]{1,0:T(8,128)(2,1)} collective-permute-done((bf16[1408,256]{1,0:T(8,128)(2,1)}, bf16[1408,256]{1,0:T(8,128)(2,1)}, u32[]{:S(2)}, u32[]{:S(2)}) %collective-permute-start.18) | collective-permute-done | bytes 720928 | tf_op jit(solution)/shard_map/ppermute | solution.py:47
  251.1 8.0 %collective-permute-done.20 = bf16[1408,256]{1,0:T(8,128)(2,1)} collective-permute-done((bf16[1408,256]{1,0:T(8,128)(2,1)}, bf16[1408,256]{1,0:T(8,128)(2,1)}, u32[]{:S(2)}, u32[]{:S(2)}) %collective-permute-start.20) | collective-permute-done | bytes 720928 | tf_op jit(solution)/shard_map/ppermute | solution.py:47
  267.7 19.4 %collective-permute-done.23 = bf16[768,512]{1,0:T(8,128)(2,1)} collective-permute-done((bf16[768,512]{1,0:T(8,128)(2,1)}, bf16[768,512]{1,0:T(8,128)(2,1)}, u32[]{:S(2)}, u32[]{:S(2)}) %collective-permute-start.23) | collective-permute-done | bytes 786464 | tf_op jit(solution)/shard_map/ppermute | solution.py:134
  287.1 3.0 add_convert_fusion.4
  292.1 2.4 collective-permute-start.25
  297.3 23.5 %collective-permute-done.25 = bf16[3,256,256]{1,2,0:T(8,128)(2,1)S(1)} collective-permute-done((bf16[3,256,256]{1,2,0:T(8,128)(2,1)S(1)}, bf16[3,256,256]{1,2,0:T(8,128)(2,1)S(1)}, u32[]{:S(2)}, u32[]{:S(2)}) %collective-permute-start.25) | collective-permute-done | bytes 393248 | tf_op jit(solution)/shard_map/ppermute | solution.py:36
  322.3 5.0 collective-permute-done.27
  329.6 9.7 %collective-permute-done.28 = bf16[3,256,256]{1,2,0:T(8,128)(2,1)S(1)} collective-permute-done((bf16[3,256,256]{1,2,0:T(8,128)(2,1)S(1)}, bf16[3,256,256]{1,2,0:T(8,128)(2,1)S(1)}, u32[]{:S(2)}, u32[]{:S(2)}) %collective-permute-start.28) | collective-permute-done | bytes 393248 | tf_op jit(solution)/shard_map/ppermute | solution.py:47
  339.4 6.0 collective-permute-done.30
  345.6 2.7 fusion.3
  353.9 6.0 all-reduce
  364.7 18.8 %collective-permute-done.33 = bf16[768,512]{1,0:T(8,128)(2,1)S(1)} collective-permute-done((bf16[768,512]{1,0:T(8,128)(2,1)S(1)}, bf16[768,512]{1,0:T(8,128)(2,1)S(1)}, u32[]{:S(2)}, u32[]{:S(2)}) %collective-permute-start.33) | collective-permute-done | bytes 786464 | tf_op jit(solution)/shard_map/ppermute | solution.py:134
  386.5 2.9 collective-permute-start.37
  391.9 2.9 broadcast.87.clone
  395.7 2.9 broadcast.87.clone.3
  399.6 4.4 collective-permute-done.34
  404.0 27.9 %collective-permute-done.35 = bf16[256,1408]{1,0:T(8,128)(2,1)S(1)} collective-permute-done((bf16[256,1408]{1,0:T(8,128)(2,1)S(1)}, bf16[256,1408]{1,0:T(8,128)(2,1)S(1)}, u32[]{:S(2)}, u32[]{:S(2)}) %collective-permute-start.35) | collective-permute-done | bytes 720928 | tf_op jit(solution)/shard_map/ppermute | solution.py:36
  435.3 15.9 %collective-permute-done.37 = bf16[256,1408]{1,0:T(8,128)(2,1)S(1)} collective-permute-done((bf16[256,1408]{1,0:T(8,128)(2,1)S(1)}, bf16[256,1408]{1,0:T(8,128)(2,1)S(1)}, u32[]{:S(2)}, u32[]{:S(2)}) %collective-permute-start.37) | collective-permute-done | bytes 720928 | tf_op jit(solution)/shard_map/ppermute | solution.py:36
  451.2 44.5 %collective-permute-done.42 = bf16[256,1408]{1,0:T(8,128)(2,1)S(1)} collective-permute-done((bf16[256,1408]{1,0:T(8,128)(2,1)S(1)}, bf16[256,1408]{1,0:T(8,128)(2,1)S(1)}, u32[]{:S(2)}, u32[]{:S(2)}) %collective-permute-start.42) | collective-permute-done | bytes 720928 | tf_op jit(solution)/shard_map/ppermute | solution.py:36
  500.6 14.2 %collective-permute-done.38 = bf16[256,1408]{1,0:T(8,128)(2,1)S(1)} collective-permute-done((bf16[256,1408]{1,0:T(8,128)(2,1)S(1)}, bf16[256,1408]{1,0:T(8,128)(2,1)S(1)}, u32[]{:S(2)}, u32[]{:S(2)}) %collective-permute-start.38) | collective-permute-done | bytes 720928 | tf_op jit(solution)/shard_map/ppermute | solution.py:47
  514.7 2.7 collective-permute-start.49
  519.9 10.3 %collective-permute-done.43 = bf16[256,1408]{1,0:T(8,128)(2,1)S(1)} collective-permute-done((bf16[256,1408]{1,0:T(8,128)(2,1)S(1)}, bf16[256,1408]{1,0:T(8,128)(2,1)S(1)}, u32[]{:S(2)}, u32[]{:S(2)}) %collective-permute-start.43) | collective-permute-done | bytes 720928 | tf_op jit(solution)/shard_map/ppermute | solution.py:47
  531.1 12.6 %collective-permute-done.46 = bf16[256,1408]{1,0:T(8,128)(2,1)S(1)} collective-permute-done((bf16[256,1408]{1,0:T(8,128)(2,1)S(1)}, bf16[256,1408]{1,0:T(8,128)(2,1)S(1)}, u32[]{:S(2)}, u32[]{:S(2)}) %collective-permute-start.46) | collective-permute-done | bytes 720928 | tf_op jit(solution)/shard_map/ppermute | solution.py:36
  548.6 14.2 %collective-permute-done.49 = bf16[1408,256]{1,0:T(8,128)(2,1)S(1)} collective-permute-done((bf16[1408,256]{1,0:T(8,128)(2,1)S(1)}, bf16[1408,256]{1,0:T(8,128)(2,1)S(1)}, u32[]{:S(2)}, u32[]{:S(2)}) %collective-permute-start.49) | collective-permute-done | bytes 720928 | tf_op jit(solution)/shard_map/ppermute | solution.py:36
  563.3 7.9 %collective-permute-done.51 = bf16[1408,256]{1,0:T(8,128)(2,1)S(1)} collective-permute-done((bf16[1408,256]{1,0:T(8,128)(2,1)S(1)}, bf16[1408,256]{1,0:T(8,128)(2,1)S(1)}, u32[]{:S(2)}, u32[]{:S(2)}) %collective-permute-start.51) | collective-permute-done | bytes 720928 | tf_op jit(solution)/shard_map/ppermute | solution.py:36
  571.8 2.9 collective-permute-done.53
  579.2 2.7 fusion.6
  582.0 7.6 %fusion.35 = f32[768,1408]{1,0:T(8,128)S(1)} fusion(bf16[2048,1408]{1,0:T(8,128)(2,1)} %constant_dynamic-update-slice_fusion.8, bf16[768,2048]{1,0:T(8,128)(2,1)S(1)} %copy-done.5, f32[2048]{0:T(1024)S(1)} %copy-done.16, f32[768]{0:T(1024)S(1)} %add_rsqrt_fusion), kind=kOutput, calls=%fused_computation.69 | convolution fusion | flops 4435476480 | bytes 13249536 | tf_op jit(solution)/shard_map/dot_general | solution.py:76
  589.7 8.3 %multiply_convert_fusion = bf16[768,1408]{1,0:T(8,128)(2,1)S(1)} fusion(f32[768,1408]{1,0:T(8,128)S(1)} %fusion.35, bf16[2048,1408]{1,0:T(8,128)(2,1)} %constant_dynamic-update-slice_fusion, bf16[768,2048]{1,0:T(8,128)(2,1)S(1)} %copy-done.5, f32[2048]{0:T(1024)S(1)} %copy-done.16, f32[768]{0:T(1024)S(1)} %add_rsqrt_fusion), kind=kOutput, calls=%fused_computation.15 | convolution fusion | flops 4441964544 | bytes 15412224 | tf_op jit(solution)/shard_map/dot_general | solution.py:77
  601.8 7.4 %collective-permute-done.50 = bf16[1408,256]{1,0:T(8,128)(2,1)} collective-permute-done((bf16[1408,256]{1,0:T(8,128)(2,1)S(1)}, bf16[1408,256]{1,0:T(8,128)(2,1)}, u32[]{:S(2)}, u32[]{:S(2)}) %collective-permute-start.50) | collective-permute-done | bytes 720928 | tf_op jit(solution)/shard_map/ppermute | solution.py:47
  611.9 12.8 %collective-permute-done.52 = bf16[1408,256]{1,0:T(8,128)(2,1)} collective-permute-done((bf16[1408,256]{1,0:T(8,128)(2,1)S(1)}, bf16[1408,256]{1,0:T(8,128)(2,1)}, u32[]{:S(2)}, u32[]{:S(2)}) %collective-permute-start.52) | collective-permute-done | bytes 720928 | tf_op jit(solution)/shard_map/ppermute | solution.py:47
  628.5 10.5 %collective-permute-done.54 = bf16[1408,256]{1,0:T(8,128)(2,1)S(1)} collective-permute-done((bf16[1408,256]{1,0:T(8,128)(2,1)}, bf16[1408,256]{1,0:T(8,128)(2,1)S(1)}, u32[]{:S(2)}, u32[]{:S(2)}) %collective-permute-start.54) | collective-permute-done | bytes 720928 | tf_op jit(solution)/shard_map/ppermute | solution.py:47
  643.5 18.8 %collective-permute-done.57 = bf16[768,512]{1,0:T(8,128)(2,1)S(1)} collective-permute-done((bf16[768,512]{1,0:T(8,128)(2,1)S(1)}, bf16[768,512]{1,0:T(8,128)(2,1)S(1)}, u32[]{:S(2)}, u32[]{:S(2)}) %collective-permute-start.57) | collective-permute-done | bytes 786464 | tf_op jit(solution)/shard_map/ppermute | solution.py:134
  (218 shorter events, 119.8 us)
Async XLA Ops:
  6.5 199.7 %all-gather.4.cloned.1.call-start = ((), (), s32[]{:S(2)}) async-start(), calls=%async_computation | async-start | bytes 3932160 | tf_op jit(solution)/shard_map/all_gather | solution.py:191
  7.3 338.3 %all-gather.6.cloned.1.call-start = ((), (), s32[]{:S(2)}) async-start(), calls=%async_computation.1 | async-start | bytes 3932160 | tf_op jit(solution)/shard_map/all_gather | solution.py:191
  8.9 33.4 %collective-permute-start.1 = (bf16[256,1408]{1,0:T(8,128)(2,1)}, bf16[256,1408]{1,0:T(8,128)(2,1)S(1)}, u32[]{:S(2)}, u32[]{:S(2)}) collective-permute-start(bf16[256,1408]{1,0:T(8,128)(2,1)} %param.17), channel_id=1, source_target_pairs={{0,8},{4,12},{8,16},{12,20},{16,24},{20,28},{24,0},{28,4},{1,9},{5... | collective-permute-start | bytes 2162696 | tf_op jit(solution)/shard_map/ppermute | solution.py:36
  10.4 113.1 %collective-permute-start.3 = (bf16[256,1408]{1,0:T(8,128)(2,1)}, bf16[256,1408]{1,0:T(8,128)(2,1)S(1)}, u32[]{:S(2)}, u32[]{:S(2)}) collective-permute-start(bf16[256,1408]{1,0:T(8,128)(2,1)} %param.17), channel_id=1, source_target_pairs={{0,16},{4,20},{8,24},{12,28},{16,0},{20,4},{24,8},{28,12},{1,17},{... | collective-permute-start | bytes 2162696 | tf_op jit(solution)/shard_map/ppermute | solution.py:36
  11.7 34.2 %collective-permute-start.7 = (bf16[256,1408]{1,0:T(8,128)(2,1)}, bf16[256,1408]{1,0:T(8,128)(2,1)}, u32[]{:S(2)}, u32[]{:S(2)}) collective-permute-start(bf16[256,1408]{1,0:T(8,128)(2,1)} %param.18), channel_id=1, source_target_pairs={{0,4},{4,0},{8,12},{12,8},{16,20},{20,16},{24,28},{28,24},{1,5},{5... | collective-permute-start | bytes 2162696 | tf_op jit(solution)/shard_map/ppermute | solution.py:47
  12.2 107.8 %collective-permute-start.8 = (bf16[256,1408]{1,0:T(8,128)(2,1)}, bf16[256,1408]{1,0:T(8,128)(2,1)S(1)}, u32[]{:S(2)}, u32[]{:S(2)}) collective-permute-start(bf16[256,1408]{1,0:T(8,128)(2,1)} %param.18), channel_id=1, source_target_pairs={{0,8},{4,12},{8,16},{12,20},{16,24},{20,28},{24,0},{28,4},{1,9},{5... | collective-permute-start | bytes 2162696 | tf_op jit(solution)/shard_map/ppermute | solution.py:36
  26.7 128.7 %collective-permute-start.5 = (bf16[256,1408]{1,0:T(8,128)(2,1)S(1)}, bf16[256,1408]{1,0:T(8,128)(2,1)S(1)}, u32[]{:S(2)}, u32[]{:S(2)}) collective-permute-start(bf16[256,1408]{1,0:T(8,128)(2,1)S(1)} %copy-done.7), channel_id=1, source_target_pairs={{0,24},{4,28},{8,0},{12,4},{16,8},{20,12},{24,16},{28,20},{1,25},{... | collective-permute-start | bytes 2162696 | tf_op jit(solution)/shard_map/ppermute | solution.py:36
  42.3 81.2 %collective-permute-start.2 = (bf16[256,1408]{1,0:T(8,128)(2,1)S(1)}, bf16[256,1408]{1,0:T(8,128)(2,1)S(1)}, u32[]{:S(2)}, u32[]{:S(2)}) collective-permute-start(bf16[256,1408]{1,0:T(8,128)(2,1)S(1)} %collective-permute-done.1), channel_id=1, source_target_pairs={{0,4},{4,0},{8,12},{12,8},{16,20},{20,16},{24,28},{28,24},{1,5},{5... | collective-permute-start | bytes 2162696 | tf_op jit(solution)/shard_map/ppermute | solution.py:47
  45.8 88.8 %collective-permute-start.10 = (bf16[256,1408]{1,0:T(8,128)(2,1)S(1)}, bf16[256,1408]{1,0:T(8,128)(2,1)S(1)}, u32[]{:S(2)}, u32[]{:S(2)}) collective-permute-start(bf16[256,1408]{1,0:T(8,128)(2,1)S(1)} %copy-done.8), channel_id=1, source_target_pairs={{0,16},{4,20},{8,24},{12,28},{16,0},{20,4},{24,8},{28,12},{1,17},{... | collective-permute-start | bytes 2162696 | tf_op jit(solution)/shard_map/ppermute | solution.py:36
  123.5 36.2 %collective-permute-start.12 = (bf16[256,1408]{1,0:T(8,128)(2,1)S(1)}, bf16[256,1408]{1,0:T(8,128)(2,1)S(1)}, u32[]{:S(2)}, u32[]{:S(2)}) collective-permute-start(bf16[256,1408]{1,0:T(8,128)(2,1)S(1)} %copy-done.8), channel_id=1, source_target_pairs={{0,24},{4,28},{8,0},{12,4},{16,8},{20,12},{24,16},{28,20},{1,25},{... | collective-permute-start | bytes 2162696 | tf_op jit(solution)/shard_map/ppermute | solution.py:36
  123.5 31.0 %collective-permute-start.4 = (bf16[256,1408]{1,0:T(8,128)(2,1)S(1)}, bf16[256,1408]{1,0:T(8,128)(2,1)S(1)}, u32[]{:S(2)}, u32[]{:S(2)}) collective-permute-start(bf16[256,1408]{1,0:T(8,128)(2,1)S(1)} %collective-permute-done.3), channel_id=1, source_target_pairs={{0,4},{4,0},{8,12},{12,8},{16,20},{20,16},{24,28},{28,24},{1,5},{5... | collective-permute-start | bytes 2162696 | tf_op jit(solution)/shard_map/ppermute | solution.py:47
  134.7 37.7 %collective-permute-start.15 = (bf16[1408,256]{1,0:T(8,128)(2,1)}, bf16[1408,256]{1,0:T(8,128)(2,1)}, u32[]{:S(2)}, u32[]{:S(2)}) collective-permute-start(bf16[1408,256]{1,0:T(8,128)(2,1)} %param.19), channel_id=1, source_target_pairs={{0,8},{4,12},{8,16},{12,20},{16,24},{20,28},{24,0},{28,4},{1,9},{5... | collective-permute-start | bytes 2162696 | tf_op jit(solution)/shard_map/ppermute | solution.py:36
  139.0 30.9 %collective-permute-start.11 = (bf16[256,1408]{1,0:T(8,128)(2,1)S(1)}, bf16[256,1408]{1,0:T(8,128)(2,1)S(1)}, u32[]{:S(2)}, u32[]{:S(2)}) collective-permute-start(bf16[256,1408]{1,0:T(8,128)(2,1)S(1)} %collective-permute-done.10), channel_id=1, source_target_pairs={{0,4},{4,0},{8,12},{12,8},{16,20},{20,16},{24,28},{28,24},{1,5},{5... | collective-permute-start | bytes 2162696 | tf_op jit(solution)/shard_map/ppermute | solution.py:47
  154.5 41.4 %collective-permute-start.17 = (bf16[1408,256]{1,0:T(8,128)(2,1)}, bf16[1408,256]{1,0:T(8,128)(2,1)}, u32[]{:S(2)}, u32[]{:S(2)}) collective-permute-start(bf16[1408,256]{1,0:T(8,128)(2,1)} %param.19), channel_id=1, source_target_pairs={{0,16},{4,20},{8,24},{12,28},{16,0},{20,4},{24,8},{28,12},{1,17},{... | collective-permute-start | bytes 2162696 | tf_op jit(solution)/shard_map/ppermute | solution.py:36
  155.4 47.0 %collective-permute-start.19 = (bf16[1408,256]{1,0:T(8,128)(2,1)}, bf16[1408,256]{1,0:T(8,128)(2,1)}, u32[]{:S(2)}, u32[]{:S(2)}) collective-permute-start(bf16[1408,256]{1,0:T(8,128)(2,1)} %param.19), channel_id=1, source_target_pairs={{0,24},{4,28},{8,0},{12,4},{16,8},{20,12},{24,16},{28,20},{1,25},{... | collective-permute-start | bytes 2162696 | tf_op jit(solution)/shard_map/ppermute | solution.py:36
  159.7 44.1 %collective-permute-start.6 = (bf16[256,1408]{1,0:T(8,128)(2,1)S(1)}, bf16[256,1408]{1,0:T(8,128)(2,1)S(1)}, u32[]{:S(2)}, u32[]{:S(2)}) collective-permute-start(bf16[256,1408]{1,0:T(8,128)(2,1)S(1)} %collective-permute-done.5), channel_id=1, source_target_pairs={{0,4},{4,0},{8,12},{12,8},{16,20},{20,16},{24,28},{28,24},{1,5},{5... | collective-permute-start | bytes 2162696 | tf_op jit(solution)/shard_map/ppermute | solution.py:47
  169.9 35.4 %collective-permute-start.13 = (bf16[256,1408]{1,0:T(8,128)(2,1)S(1)}, bf16[256,1408]{1,0:T(8,128)(2,1)S(1)}, u32[]{:S(2)}, u32[]{:S(2)}) collective-permute-start(bf16[256,1408]{1,0:T(8,128)(2,1)S(1)} %collective-permute-done.12), channel_id=1, source_target_pairs={{0,4},{4,0},{8,12},{12,8},{16,20},{20,16},{24,28},{28,24},{1,5},{5... | collective-permute-start | bytes 2162696 | tf_op jit(solution)/shard_map/ppermute | solution.py:47
  172.3 54.9 %collective-permute-start.14 = (bf16[1408,256]{1,0:T(8,128)(2,1)}, bf16[1408,256]{1,0:T(8,128)(2,1)}, u32[]{:S(2)}, u32[]{:S(2)}) collective-permute-start(bf16[1408,256]{1,0:T(8,128)(2,1)} %param.19), channel_id=1, source_target_pairs={{0,4},{4,0},{8,12},{12,8},{16,20},{20,16},{24,28},{28,24},{1,5},{5... | collective-permute-start | bytes 2162696 | tf_op jit(solution)/shard_map/ppermute | solution.py:47
  195.9 36.0 %collective-permute-start.16 = (bf16[1408,256]{1,0:T(8,128)(2,1)}, bf16[1408,256]{1,0:T(8,128)(2,1)}, u32[]{:S(2)}, u32[]{:S(2)}) collective-permute-start(bf16[1408,256]{1,0:T(8,128)(2,1)} %collective-permute-done.15), channel_id=1, source_target_pairs={{0,4},{4,0},{8,12},{12,8},{16,20},{20,16},{24,28},{28,24},{1,5},{5... | collective-permute-start | bytes 2162696 | tf_op jit(solution)/shard_map/ppermute | solution.py:47
  202.4 44.9 %collective-permute-start.18 = (bf16[1408,256]{1,0:T(8,128)(2,1)}, bf16[1408,256]{1,0:T(8,128)(2,1)}, u32[]{:S(2)}, u32[]{:S(2)}) collective-permute-start(bf16[1408,256]{1,0:T(8,128)(2,1)} %collective-permute-done.17), channel_id=1, source_target_pairs={{0,4},{4,0},{8,12},{12,8},{16,20},{20,16},{24,28},{28,24},{1,5},{5... | collective-permute-start | bytes 2162696 | tf_op jit(solution)/shard_map/ppermute | solution.py:47
  203.8 55.2 %collective-permute-start.20 = (bf16[1408,256]{1,0:T(8,128)(2,1)}, bf16[1408,256]{1,0:T(8,128)(2,1)}, u32[]{:S(2)}, u32[]{:S(2)}) collective-permute-start(bf16[1408,256]{1,0:T(8,128)(2,1)} %collective-permute-done.19), channel_id=1, source_target_pairs={{0,4},{4,0},{8,12},{12,8},{16,20},{20,16},{24,28},{28,24},{1,5},{5... | collective-permute-start | bytes 2162696 | tf_op jit(solution)/shard_map/ppermute | solution.py:47
  267.2 19.9 %collective-permute-start.23 = (bf16[768,512]{1,0:T(8,128)(2,1)}, bf16[768,512]{1,0:T(8,128)(2,1)}, u32[]{:S(2)}, u32[]{:S(2)}) collective-permute-start(bf16[768,512]{1,0:T(8,128)(2,1)} %add_convert_fusion.5), channel_id=1, source_target_pairs={{0,2},{1,3},{2,0},{3,1},{4,6},{5,7},{6,4},{7,5},{8,10},{9,11},{10,... | collective-permute-start | bytes 2359304 | tf_op jit(solution)/shard_map/ppermute | solution.py:134
  290.1 289.1 %all-gather.8.cloned.1.call-start = ((), (), s32[]{:S(2)}) async-start(), calls=%async_computation.2 | async-start | bytes 3932160 | tf_op jit(solution)/shard_map/all_gather | solution.py:191
  291.5 37.9 %collective-permute-start.24 = (bf16[3,256,256]{1,2,0:T(8,128)(2,1)S(1)}, bf16[3,256,256]{1,2,0:T(8,128)(2,1)S(1)}, u32[]{:S(2)}, u32[]{:S(2)}) collective-permute-start(bf16[3,256,256]{1,2,0:T(8,128)(2,1)S(1)} %pad_maximum_fusion), channel_id=1, source_target_pairs={{0,4},{4,0},{8,12},{12,8},{16,20},{20,16},{24,28},{28,24},{1,5},{5... | collective-permute-start | bytes 1179656 | tf_op jit(solution)/shard_map/ppermute | solution.py:47
  292.1 28.7 %collective-permute-start.25 = (bf16[3,256,256]{1,2,0:T(8,128)(2,1)S(1)}, bf16[3,256,256]{1,2,0:T(8,128)(2,1)S(1)}, u32[]{:S(2)}, u32[]{:S(2)}) collective-permute-start(bf16[3,256,256]{1,2,0:T(8,128)(2,1)S(1)} %pad_maximum_fusion), channel_id=1, source_target_pairs={{0,8},{4,12},{8,16},{12,20},{16,24},{20,28},{24,0},{28,4},{1,9},{5... | collective-permute-start | bytes 1179656 | tf_op jit(solution)/shard_map/ppermute | solution.py:36
  294.5 32.8 %collective-permute-start.27 = (bf16[3,256,256]{1,2,0:T(8,128)(2,1)S(1)}, bf16[3,256,256]{1,2,0:T(8,128)(2,1)S(1)}, u32[]{:S(2)}, u32[]{:S(2)}) collective-permute-start(bf16[3,256,256]{1,2,0:T(8,128)(2,1)S(1)} %pad_maximum_fusion), channel_id=1, source_target_pairs={{0,16},{4,20},{8,24},{12,28},{16,0},{20,4},{24,8},{28,12},{1,17},{... | collective-permute-start | bytes 1179656 | tf_op jit(solution)/shard_map/ppermute | solution.py:36
  294.5 34.3 %collective-permute-start.29 = (bf16[3,256,256]{1,2,0:T(8,128)(2,1)S(1)}, bf16[3,256,256]{1,2,0:T(8,128)(2,1)S(1)}, u32[]{:S(2)}, u32[]{:S(2)}) collective-permute-start(bf16[3,256,256]{1,2,0:T(8,128)(2,1)S(1)} %pad_maximum_fusion), channel_id=1, source_target_pairs={{0,24},{4,28},{8,0},{12,4},{16,8},{20,12},{24,16},{28,20},{1,25},{... | collective-permute-start | bytes 1179656 | tf_op jit(solution)/shard_map/ppermute | solution.py:36
  363.8 19.6 %collective-permute-start.33 = (bf16[768,512]{1,0:T(8,128)(2,1)S(1)}, bf16[768,512]{1,0:T(8,128)(2,1)S(1)}, u32[]{:S(2)}, u32[]{:S(2)}) collective-permute-start(bf16[768,512]{1,0:T(8,128)(2,1)S(1)} %add_convert_fusion.3), channel_id=1, source_target_pairs={{0,2},{1,3},{2,0},{3,1},{4,6},{5,7},{6,4},{7,5},{8,10},{9,11},{10,... | collective-permute-start | bytes 2359304 | tf_op jit(solution)/shard_map/ppermute | solution.py:134
  386.5 45.5 %collective-permute-start.35 = (bf16[256,1408]{1,0:T(8,128)(2,1)S(1)}, bf16[256,1408]{1,0:T(8,128)(2,1)S(1)}, u32[]{:S(2)}, u32[]{:S(2)}) collective-permute-start(bf16[256,1408]{1,0:T(8,128)(2,1)S(1)} %copy-done.9), channel_id=1, source_target_pairs={{0,8},{4,12},{8,16},{12,20},{16,24},{20,28},{24,0},{28,4},{1,9},{5... | collective-permute-start | bytes 2162696 | tf_op jit(solution)/shard_map/ppermute | solution.py:36
  386.5 64.7 %collective-permute-start.37 = (bf16[256,1408]{1,0:T(8,128)(2,1)S(1)}, bf16[256,1408]{1,0:T(8,128)(2,1)S(1)}, u32[]{:S(2)}, u32[]{:S(2)}) collective-permute-start(bf16[256,1408]{1,0:T(8,128)(2,1)S(1)} %copy-done.9), channel_id=1, source_target_pairs={{0,16},{4,20},{8,24},{12,28},{16,0},{20,4},{24,8},{28,12},{1,17},{... | collective-permute-start | bytes 2162696 | tf_op jit(solution)/shard_map/ppermute | solution.py:36
  389.3 129.0 %collective-permute-start.39 = (bf16[256,1408]{1,0:T(8,128)(2,1)S(1)}, bf16[256,1408]{1,0:T(8,128)(2,1)S(1)}, u32[]{:S(2)}, u32[]{:S(2)}) collective-permute-start(bf16[256,1408]{1,0:T(8,128)(2,1)S(1)} %copy-done.9), channel_id=1, source_target_pairs={{0,24},{4,28},{8,0},{12,4},{16,8},{20,12},{24,16},{28,20},{1,25},{... | collective-permute-start | bytes 2162696 | tf_op jit(solution)/shard_map/ppermute | solution.py:36
  391.4 43.0 %collective-permute-start.41 = (bf16[256,1408]{1,0:T(8,128)(2,1)S(1)}, bf16[256,1408]{1,0:T(8,128)(2,1)S(1)}, u32[]{:S(2)}, u32[]{:S(2)}) collective-permute-start(bf16[256,1408]{1,0:T(8,128)(2,1)S(1)} %copy-done.10), channel_id=1, source_target_pairs={{0,4},{4,0},{8,12},{12,8},{16,20},{20,16},{24,28},{28,24},{1,5},{5... | collective-permute-start | bytes 2162696 | tf_op jit(solution)/shard_map/ppermute | solution.py:47
  404.0 91.7 %collective-permute-start.42 = (bf16[256,1408]{1,0:T(8,128)(2,1)S(1)}, bf16[256,1408]{1,0:T(8,128)(2,1)S(1)}, u32[]{:S(2)}, u32[]{:S(2)}) collective-permute-start(bf16[256,1408]{1,0:T(8,128)(2,1)S(1)} %copy-done.10), channel_id=1, source_target_pairs={{0,8},{4,12},{8,16},{12,20},{16,24},{20,28},{24,0},{28,4},{1,9},{5... | collective-permute-start | bytes 2162696 | tf_op jit(solution)/shard_map/ppermute | solution.py:36
  431.9 65.3 %collective-permute-start.36 = (bf16[256,1408]{1,0:T(8,128)(2,1)S(1)}, bf16[256,1408]{1,0:T(8,128)(2,1)S(1)}, u32[]{:S(2)}, u32[]{:S(2)}) collective-permute-start(bf16[256,1408]{1,0:T(8,128)(2,1)S(1)} %collective-permute-done.35), channel_id=1, source_target_pairs={{0,4},{4,0},{8,12},{12,8},{16,20},{20,16},{24,28},{28,24},{1,5},{5... | collective-permute-start | bytes 2162696 | tf_op jit(solution)/shard_map/ppermute | solution.py:47
  434.3 84.0 %collective-permute-start.44 = (bf16[256,1408]{1,0:T(8,128)(2,1)S(1)}, bf16[256,1408]{1,0:T(8,128)(2,1)S(1)}, u32[]{:S(2)}, u32[]{:S(2)}) collective-permute-start(bf16[256,1408]{1,0:T(8,128)(2,1)S(1)} %copy-done.10), channel_id=1, source_target_pairs={{0,16},{4,20},{8,24},{12,28},{16,0},{20,4},{24,8},{28,12},{1,17},{... | collective-permute-start | bytes 2162696 | tf_op jit(solution)/shard_map/ppermute | solution.py:36
  451.2 92.6 %collective-permute-start.46 = (bf16[256,1408]{1,0:T(8,128)(2,1)S(1)}, bf16[256,1408]{1,0:T(8,128)(2,1)S(1)}, u32[]{:S(2)}, u32[]{:S(2)}) collective-permute-start(bf16[256,1408]{1,0:T(8,128)(2,1)S(1)} %copy-done.10), channel_id=1, source_target_pairs={{0,24},{4,28},{8,0},{12,4},{16,8},{20,12},{24,16},{28,20},{1,25},{... | collective-permute-start | bytes 2162696 | tf_op jit(solution)/shard_map/ppermute | solution.py:36
  497.2 33.0 %collective-permute-start.43 = (bf16[256,1408]{1,0:T(8,128)(2,1)S(1)}, bf16[256,1408]{1,0:T(8,128)(2,1)S(1)}, u32[]{:S(2)}, u32[]{:S(2)}) collective-permute-start(bf16[256,1408]{1,0:T(8,128)(2,1)S(1)} %collective-permute-done.42), channel_id=1, source_target_pairs={{0,4},{4,0},{8,12},{12,8},{16,20},{20,16},{24,28},{28,24},{1,5},{5... | collective-permute-start | bytes 2162696 | tf_op jit(solution)/shard_map/ppermute | solution.py:47
  514.7 48.1 %collective-permute-start.49 = (bf16[1408,256]{1,0:T(8,128)(2,1)S(1)}, bf16[1408,256]{1,0:T(8,128)(2,1)S(1)}, u32[]{:S(2)}, u32[]{:S(2)}) collective-permute-start(bf16[1408,256]{1,0:T(8,128)(2,1)S(1)} %copy-done.13), channel_id=1, source_target_pairs={{0,8},{4,12},{8,16},{12,20},{16,24},{20,28},{24,0},{28,4},{1,9},{5... | collective-permute-start | bytes 2162696 | tf_op jit(solution)/shard_map/ppermute | solution.py:36
  518.4 52.9 %collective-permute-start.51 = (bf16[1408,256]{1,0:T(8,128)(2,1)S(1)}, bf16[1408,256]{1,0:T(8,128)(2,1)S(1)}, u32[]{:S(2)}, u32[]{:S(2)}) collective-permute-start(bf16[1408,256]{1,0:T(8,128)(2,1)S(1)} %copy-done.13), channel_id=1, source_target_pairs={{0,16},{4,20},{8,24},{12,28},{16,0},{20,4},{24,8},{28,12},{1,17},{... | collective-permute-start | bytes 2162696 | tf_op jit(solution)/shard_map/ppermute | solution.py:36
  518.4 26.9 %collective-permute-start.45 = (bf16[256,1408]{1,0:T(8,128)(2,1)S(1)}, bf16[256,1408]{1,0:T(8,128)(2,1)S(1)}, u32[]{:S(2)}, u32[]{:S(2)}) collective-permute-start(bf16[256,1408]{1,0:T(8,128)(2,1)S(1)} %collective-permute-done.44), channel_id=1, source_target_pairs={{0,4},{4,0},{8,12},{12,8},{16,20},{20,16},{24,28},{28,24},{1,5},{5... | collective-permute-start | bytes 2162696 | tf_op jit(solution)/shard_map/ppermute | solution.py:47
  530.2 44.5 %collective-permute-start.53 = (bf16[1408,256]{1,0:T(8,128)(2,1)S(1)}, bf16[1408,256]{1,0:T(8,128)(2,1)}, u32[]{:S(2)}, u32[]{:S(2)}) collective-permute-start(bf16[1408,256]{1,0:T(8,128)(2,1)S(1)} %copy-done.13), channel_id=1, source_target_pairs={{0,24},{4,28},{8,0},{12,4},{16,8},{20,12},{24,16},{28,20},{1,25},{... | collective-permute-start | bytes 2162696 | tf_op jit(solution)/shard_map/ppermute | solution.py:36
  543.8 31.5 %collective-permute-start.40 = (bf16[256,1408]{1,0:T(8,128)(2,1)S(1)}, bf16[256,1408]{1,0:T(8,128)(2,1)S(1)}, u32[]{:S(2)}, u32[]{:S(2)}) collective-permute-start(bf16[256,1408]{1,0:T(8,128)(2,1)S(1)} %collective-permute-done.39), channel_id=1, source_target_pairs={{0,4},{4,0},{8,12},{12,8},{16,20},{20,16},{24,28},{28,24},{1,5},{5... | collective-permute-start | bytes 2162696 | tf_op jit(solution)/shard_map/ppermute | solution.py:47
  545.2 33.0 %collective-permute-start.47 = (bf16[256,1408]{1,0:T(8,128)(2,1)S(1)}, bf16[256,1408]{1,0:T(8,128)(2,1)S(1)}, u32[]{:S(2)}, u32[]{:S(2)}) collective-permute-start(bf16[256,1408]{1,0:T(8,128)(2,1)S(1)} %collective-permute-done.46), channel_id=1, source_target_pairs={{0,4},{4,0},{8,12},{12,8},{16,20},{20,16},{24,28},{28,24},{1,5},{5... | collective-permute-start | bytes 2162696 | tf_op jit(solution)/shard_map/ppermute | solution.py:47
  562.8 36.3 %collective-permute-start.48 = (bf16[1408,256]{1,0:T(8,128)(2,1)S(1)}, bf16[1408,256]{1,0:T(8,128)(2,1)}, u32[]{:S(2)}, u32[]{:S(2)}) collective-permute-start(bf16[1408,256]{1,0:T(8,128)(2,1)S(1)} %copy-done.13), channel_id=1, source_target_pairs={{0,4},{4,0},{8,12},{12,8},{16,20},{20,16},{24,28},{28,24},{1,5},{5... | collective-permute-start | bytes 2162696 | tf_op jit(solution)/shard_map/ppermute | solution.py:47
  571.3 38.0 %collective-permute-start.50 = (bf16[1408,256]{1,0:T(8,128)(2,1)S(1)}, bf16[1408,256]{1,0:T(8,128)(2,1)}, u32[]{:S(2)}, u32[]{:S(2)}) collective-permute-start(bf16[1408,256]{1,0:T(8,128)(2,1)S(1)} %collective-permute-done.49), channel_id=1, source_target_pairs={{0,4},{4,0},{8,12},{12,8},{16,20},{20,16},{24,28},{28,24},{1,5},{5... | collective-permute-start | bytes 2162696 | tf_op jit(solution)/shard_map/ppermute | solution.py:47
  574.7 50.0 %collective-permute-start.52 = (bf16[1408,256]{1,0:T(8,128)(2,1)S(1)}, bf16[1408,256]{1,0:T(8,128)(2,1)}, u32[]{:S(2)}, u32[]{:S(2)}) collective-permute-start(bf16[1408,256]{1,0:T(8,128)(2,1)S(1)} %collective-permute-done.51), channel_id=1, source_target_pairs={{0,4},{4,0},{8,12},{12,8},{16,20},{20,16},{24,28},{28,24},{1,5},{5... | collective-permute-start | bytes 2162696 | tf_op jit(solution)/shard_map/ppermute | solution.py:47
  575.3 63.8 %collective-permute-start.54 = (bf16[1408,256]{1,0:T(8,128)(2,1)}, bf16[1408,256]{1,0:T(8,128)(2,1)S(1)}, u32[]{:S(2)}, u32[]{:S(2)}) collective-permute-start(bf16[1408,256]{1,0:T(8,128)(2,1)} %collective-permute-done.53), channel_id=1, source_target_pairs={{0,4},{4,0},{8,12},{12,8},{16,20},{20,16},{24,28},{28,24},{1,5},{5... | collective-permute-start | bytes 2162696 | tf_op jit(solution)/shard_map/ppermute | solution.py:47
  642.6 19.6 %collective-permute-start.57 = (bf16[768,512]{1,0:T(8,128)(2,1)S(1)}, bf16[768,512]{1,0:T(8,128)(2,1)S(1)}, u32[]{:S(2)}, u32[]{:S(2)}) collective-permute-start(bf16[768,512]{1,0:T(8,128)(2,1)S(1)} %add_convert_fusion.1), channel_id=1, source_target_pairs={{0,2},{1,3},{2,0},{3,1},{4,6},{5,7},{6,4},{7,5},{8,10},{9,11},{10,... | collective-permute-start | bytes 2359304 | tf_op jit(solution)/shard_map/ppermute | solution.py:134
  (32 other events, 849.2 us)
Sparse Core Ops, SparseCore 0:
  8.9 28.6 all-gather.3
  290.2 27.5 all-gather.5
  385.0 28.9 all-gather.7
